TPU v7x, 512 devices: a 4x2x32 block of a 4x8x32 slice. The times are simulated.
512 devices in a mesh: grp: 2 (over y), ep: 64 (over z, core), tp: 4 (over x).
Axes of the slice: x: 4, y: 2, z: 32, core: 2. Of those that a mesh axis runs over, the one named last changes fastest.
The devices are a block of a 4x8x32 slice.
Arguments:
- tokens: bfloat16 [49152, 2048], P(('grp', 'ep'), 'tp'), parts along dimension 0
- group_choice: int32 [49152], P(('grp', 'ep')), parts along dimension 0, may hold values from 0 to 7, as said below
- expert_choice: int32 [49152, 2], P(('grp', 'ep')), parts along dimension 0, may hold values from 0 to 7, as said below
- group_weight: float32 [49152], P(('grp', 'ep')), parts along dimension 0, may hold values from 0.3 to 1
- expert_weight: float32 [49152, 2], P(('grp', 'ep')), parts along dimension 0, may hold values from 0.1 to 1
- norm_gain: float32 [2048], replicated, may hold values from 0.1 to 1.9
- w_gate: bfloat16 [64, 2048, 1024], P('ep', None, 'tp'), may hold values from -0.125 to 0.125
- w_up: bfloat16 [64, 2048, 1024], P('ep', None, 'tp'), may hold values from -0.125 to 0.125
- w_down: bfloat16 [64, 1024, 2048], P('ep', None, 'tp'), may hold values from -0.1875 to 0.1875
Outputs:
- moe_out: bfloat16 [49152, 2048], P(('grp', 'ep'), 'tp'), parts along dimension 0
There are 2 independent parts, one for each index of `grp`. A program takes and returns all parts, laid end to end along the dimension named above; an argument that names none is the same for every part. Nothing has to cross between parts.
Inputs may be any that keep to these rules, and one draw needn't show every extreme that they name: `group_choice`: group of each token, 0 to 7; within each aligned block of 384 tokens (the tokens of one index of ep) every group is chosen by the same number of tokens. `expert_choice`: a token's two entries differ; within each aligned block of 384 tokens no expert (group with entry) is named by more than 18 tokens, and in every block one expert of each group, the same one in all blocks, is named by exactly 18 tokens.
All inputs are finite; a program needn't handle non-finite values.
Results may differ from a plain program's by a relative error of at most 0.0071.
Values may be sent and summed in bfloat16 or wider, within the bound.
A program may use at most 64 MiB of HBM per device.

v0:
```python
import jax
import jax.numpy as jnp
from jax import lax
from jax.sharding import Mesh
from jax.sharding import PartitionSpec as P

EP = ("ep_0", "ep_1")
GRP_EP = ("grp", "ep_0", "ep_1")


def copy_for_each(array, axis):
    length = lax.axis_size(axis)
    return lax.all_to_all(
        jnp.broadcast_to(array[None], (length, *array.shape)), axis, 0, 0, tiled=True
    )


def laid_out(blocks, dim):
    dims = list(blocks.shape[1:])
    dims[dim] *= blocks.shape[0]
    return jnp.moveaxis(blocks, 0, dim).reshape(dims)


def collect(array, axis, dim):
    blocks = copy_for_each(array, axis)
    return laid_out(blocks, dim)


def over_copies(array, axis):
    everything = copy_for_each(array, axis)
    return jnp.sum(everything, axis=0)


def cut_along(array, dim, length):
    dims = array.shape
    blocks = array.reshape(*dims[:dim], length, dims[dim] // length, *dims[dim + 1 :])
    return jnp.moveaxis(blocks, dim, 0)


def moved_by_axis(blocks, axes, turns):
    dims = [lax.axis_size(a) for a in axes]
    blocks = blocks.reshape(*dims, *blocks.shape[1:])
    for k in turns:
        blocks = lax.all_to_all(blocks, axes[k], split_axis=k, concat_axis=k, tiled=True)
    return blocks.reshape(-1, *blocks.shape[len(axes) :])


def exchange_by_chip(array, groups, turns, split_dim, concat_dim):
    length = lax.axis_size(groups[0]) * lax.axis_size(groups[1])
    blocks = cut_along(array, split_dim, length)
    return laid_out(moved_by_axis(blocks, groups, turns), concat_dim)


def finish_rows(gate_sum, up_sum, w_down):
    hidden = (jax.nn.silu(gate_sum) * up_sum).astype(jnp.bfloat16)
    whole_hidden = collect(hidden, "tp", 3)
    summed = jnp.einsum("sxcf,xfd->sxcd", whole_hidden, w_down, preferred_element_type=jnp.float32)
    return summed.astype(jnp.bfloat16)


def body(
    tokens,
    group_choice,
    expert_choice,
    group_weight,
    expert_weight,
    norm_gain,
    w_gate,
    w_up,
    w_down,
):
    tok_rows = tokens.shape[0]
    ep_count = lax.axis_size(EP)
    exp_local = w_gate.shape[0]
    experts_all = ep_count * exp_local
    group_size = min(8, experts_all // 2)
    group_count = experts_all // group_size
    mean_load = 2 * tok_rows // experts_all
    capacity = mean_load + min(mean_load // 2, tok_rows // group_count - mean_load)
    model_width = norm_gain.shape[0]
    expert_ids = group_choice[:, None] * group_size + expert_choice
    mixing = group_weight[:, None] * expert_weight / jnp.sum(expert_weight, -1, keepdims=True)
    flat_ids = expert_ids.reshape(-1)
    marks = (flat_ids[:, None] == jnp.arange(experts_all, dtype=jnp.int32)[None, :]).astype(
        jnp.int32
    )
    earlier = jnp.cumsum(marks, 0) - marks
    seat_index = jnp.sum(earlier * marks, 1)
    targets = (flat_ids * capacity + seat_index).reshape(tok_rows, 2)
    places = jnp.arange(experts_all * capacity, dtype=jnp.int32)
    dispatch = (
        (places[:, None] == targets[None, :, 0]) | (places[:, None] == targets[None, :, 1])
    ).astype(jnp.bfloat16)
    values = tokens.astype(jnp.float32)
    own_squares = jnp.sum(values * values, -1)
    all_squares = over_copies(own_squares, "tp")
    inv_rms = lax.rsqrt(all_squares / model_width + 1e-06)
    piece_width = tokens.shape[1]
    gain_piece = lax.dynamic_slice_in_dim(
        norm_gain, lax.axis_index("tp") * piece_width, piece_width, 0
    )
    normed = (values * inv_rms[:, None] * gain_piece[None, :]).astype(jnp.bfloat16)
    buffer = jnp.dot(dispatch, normed, preferred_element_type=jnp.float32).astype(jnp.bfloat16)
    buffer = buffer.reshape(ep_count, exp_local, capacity, piece_width)
    piece = lax.all_gather(
        lax.all_to_all(buffer, EP, split_axis=0, concat_axis=0, tiled=True),
        "tp",
        axis=3,
        tiled=True,
    )
    gate_next = jnp.einsum("sxcd,xdf->sxcf", piece, w_gate, preferred_element_type=jnp.float32)
    up_next = jnp.einsum("sxcd,xdf->sxcf", piece, w_up, preferred_element_type=jnp.float32)
    results = finish_rows(gate_next, up_next, w_down)
    returned = exchange_by_chip(results, ("ep_0", "ep_1"), (1, 0), 0, 0)
    returned = returned.reshape(experts_all * capacity, returned.shape[3])
    combined = jnp.zeros((tok_rows, returned.shape[1]), jnp.float32)
    for choice_index in range(2):
        picker = (targets[:, choice_index : choice_index + 1] == places[None, :]).astype(
            jnp.bfloat16
        )
        picked = jnp.dot(picker, returned, preferred_element_type=jnp.float32)
        combined = combined + mixing[:, choice_index : choice_index + 1] * picked
    return combined.astype(jnp.bfloat16)


def solution(mesh):
    split = Mesh(
        mesh.devices.reshape(mesh.shape["grp"], 32, 2, mesh.shape["tp"]),
        ("grp", "ep_0", "ep_1", "tp"),
    )
    placed = (
        P(GRP_EP, "tp"),
        P(GRP_EP),
        P(GRP_EP, None),
        P(GRP_EP),
        P(GRP_EP, None),
        P(),
        P(EP, None, "tp"),
        P(EP, None, "tp"),
        P(EP, None, "tp"),
    )
    return jax.shard_map(
        body, mesh=split, in_specs=placed, out_specs=P(GRP_EP, "tp"), check_vma=False
    )
```

profile of v0, /device:TPU:33, one launch (start us, length us, event | category | flops | bytes accessed | tf_op | source)
XLA Modules:
  0.0 482.4 jit_solution(356377158643691526)
XLA Ops:
  6.5 0.0 copy-start
  6.6 1.2 fusion.35
  7.8 0.6 broadcast_in_dim.6
  8.4 5.1 %all-to-all-start = ((f32[4,1,384]{2,1,0:T(1,128)}), f32[4,1,384]{2,1,0:T(1,128)S(1)}, u32[]{:S(2)}, u32[]{:S(2)}) async-start(f32[4,1,384]{2,1,0:T(1,128)} %broadcast_in_dim.6), calls=%async_computation | async-start | bytes 12288 | tf_op jit(solution)/shard_map/all_to_all | solution.py:13
  13.5 0.0 all-gather.2.cloned.1.call-start
  13.5 0.8 copy.35
  14.3 0.7 broadcast_multiply_fusion
  15.0 0.1 broadcast_add_fusion
  15.1 0.1 eq.85
  15.3 0.0 copy-start.2
  15.3 0.1 eq.81
  15.5 1.8 reduce-window.6
  17.3 0.3 slice_reduce_fusion.2
  17.6 0.1 fusion.43
  17.7 0.2 reduce_sum.40
  17.9 0.1 multiply_add_fusion
  18.0 0.3 slice_reduce_fusion.1
  18.3 0.8 dynamic_slice.3
  19.0 0.0 all-to-all-done
  19.1 0.0 copy-done.2
  19.1 1.9 convolution_convert_fusion
  21.0 2.2 reshape.67
  23.2 199.5 %all_to_all.26 = bf16[64,1,18,512]{3,2,1,0:T(8,128)(2,1)S(1)} all-to-all(bf16[64,1,18,512]{3,2,1,0:T(8,128)(2,1)S(1)} %bitcast.87), channel_id=1, replica_groups=mesh['grp'=2,'ep_0'=32,'ep_1'=2,'tp'=4] {'ep_0','ep_1'}, dimensions={0} | all-to-all | bytes 2359296 | tf_op jit(solution)/shard_map/all_to_all | solution.py:106
  222.7 1.4 copy.39
  224.1 0.1 all-gather.2.cloned.1.call-update
  224.2 0.0 copy-start.7
  224.2 52.9 %all-gather.2.cloned.1.call-done = bf16[64,1,18,2048]{3,0,2,1:T(8,128)(2,1)} async-done(((bf16[64,1,18,512]{3,0,2,1:T(8,128)(2,1)}), bf16[64,1,18,2048]{3,0,2,1:T(8,128)(2,1)}) %all-gather.2.cloned.1.call-update) | async-done | bytes 4718608 | tf_op jit(solution)/shard_map/all_gather | solution.py:105
  277.1 0.0 copy-done.6
  277.1 3.9 fusion.9
  281.0 0.0 copy-done.7
  281.0 1.5 fusion.25
  282.5 0.3 broadcast_in_dim.8
  282.8 31.1 %all_to_all.27 = bf16[4,64,1,18,256]{4,1,3,2,0:T(8,128)(2,1)S(1)} all-to-all(bf16[4,64,1,18,256]{4,1,3,2,0:T(8,128)(2,1)S(1)} %broadcast_in_dim.8), channel_id=1, replica_groups=mesh['grp'=2,'ep_0'=32,'ep_1'=2,'tp'=4] {'tp'}, dimensions={0} | all-to-all | bytes 4718592 | tf_op jit(solution)/shard_map/all_to_all | solution.py:13
  313.9 2.0 copy.40
  315.9 2.9 reshape.71
  318.8 3.0 fusion.8
  321.9 0.5 reshape_reshape.3
  322.4 0.2 copy.41
  322.6 6.3 %all_to_all.28 = bf16[32,2,1,1,18,512]{5,0,4,3,2,1:T(8,128)(2,1)S(1)} all-to-all(bf16[32,2,1,1,18,512]{5,0,4,3,2,1:T(8,128)(2,1)S(1)} %copy.41), channel_id=1, replica_groups=mesh['grp'=2,'ep_0'=32,'ep_1'=2,'tp'=4] {'ep_1'}, dimensions={1} | all-to-all | bytes 2359296 | tf_op jit(solution)/shard_map/all_to_all | solution.py:44
  328.9 2.3 copy.42
  331.2 23.3 %all-to-all-start.4 = ((bf16[32,2,1,1,18,512]{5,1,4,3,2,0:T(2,128)(2,1)}), bf16[32,2,1,1,18,512]{5,1,4,3,2,0:T(2,128)(2,1)}, u32[]{:S(2)}, u32[]{:S(2)}) async-start(bf16[32,2,1,1,18,512]{5,1,4,3,2,0:T(2,128)(2,1)} %copy.42), calls=%async_computation.4 | async-start | bytes 2359296 | tf_op jit(solution)/shard_map/all_to_all | solution.py:44
  354.6 0.0 copy-done.4
  354.6 114.5 %all-to-all-done.4 = bf16[32,2,1,1,18,512]{5,1,4,3,2,0:T(2,128)(2,1)} async-done(((bf16[32,2,1,1,18,512]{5,1,4,3,2,0:T(2,128)(2,1)}), bf16[32,2,1,1,18,512]{5,1,4,3,2,0:T(2,128)(2,1)}, u32[]{:S(2)}, u32[]{:S(2)}) %all-to-all-start.4) | async-done | bytes 1179680 | tf_op jit(solution)/shard_map/all_to_all | solution.py:44
  469.1 1.6 copy.43
  470.7 1.2 reshape_reshape_reshape.3
  472.0 2.1 fusion.23
  474.0 0.0 copy-done.1
  474.0 1.5 fusion.24
  (15 shorter events, 0.1 us)
Async XLA Ops:
  6.5 312.3 %copy-start = (bf16[1,1024,512]{2,1,0:T(8,128)(2,1)S(1)}, bf16[1,1024,512]{2,1,0:T(8,128)(2,1)}, u32[]{:S(2)}) copy-start(bf16[1,1024,512]{2,1,0:T(8,128)(2,1)} %param.17) | copy-start | bytes 3145732
  8.4 10.6 %all-to-all-start = ((f32[4,1,384]{2,1,0:T(1,128)}), f32[4,1,384]{2,1,0:T(1,128)S(1)}, u32[]{:S(2)}, u32[]{:S(2)}) async-start(f32[4,1,384]{2,1,0:T(1,128)} %broadcast_in_dim.6), calls=%async_computation | async-start | bytes 12288 | tf_op jit(solution)/shard_map/all_to_all | solution.py:13
  13.5 263.6 %all-gather.2.cloned.1.call-start = ((), (), s32[]{:S(2)}) async-start(), calls=%async_computation.5 | async-start | bytes 5898240 | tf_op jit(solution)/shard_map/all_gather | solution.py:105
  15.3 3.8 copy-start.2
  224.1 53.0 %copy-start.6 = (bf16[1,2048,256]{2,1,0:T(8,128)(2,1)S(1)}, bf16[1,2048,256]{2,1,0:T(8,128)(2,1)}, u32[]{:S(2)}) copy-start(bf16[1,2048,256]{2,1,0:T(8,128)(2,1)} %param.15) | copy-start | bytes 3145732
  224.2 56.8 %copy-start.7 = (bf16[1,2048,256]{2,1,0:T(8,128)(2,1)S(1)}, bf16[1,2048,256]{2,1,0:T(8,128)(2,1)}, u32[]{:S(2)}) copy-start(bf16[1,2048,256]{2,1,0:T(8,128)(2,1)} %param.16) | copy-start | bytes 3145732
  277.1 3.9 copy-start.5
  331.2 23.4 %copy-start.3 = (f32[384,2]{0,1:T(2,128)S(1)}, f32[384,2]{0,1:T(2,128)}, u32[]{:S(2)}) copy-start(f32[384,2]{0,1:T(2,128)} %param.13) | copy-start | bytes 9220
  331.2 23.4 %copy-start.4 = (f32[384]{0:T(512)S(1)}, f32[384]{0:T(512)}, u32[]{:S(2)}) copy-start(f32[384]{0:T(512)} %param.12) | copy-start | bytes 4612
  331.2 137.9 %all-to-all-start.4 = ((bf16[32,2,1,1,18,512]{5,1,4,3,2,0:T(2,128)(2,1)}), bf16[32,2,1,1,18,512]{5,1,4,3,2,0:T(2,128)(2,1)}, u32[]{:S(2)}, u32[]{:S(2)}) async-start(bf16[32,2,1,1,18,512]{5,1,4,3,2,0:T(2,128)(2,1)} %copy.42), calls=%async_computation.4 | async-start | bytes 2359296 | tf_op jit(solution)/shard_map/all_to_all | solution.py:44
  472.0 2.1 copy-start.1
Sparse Core Ops, SparseCore 0:
  224.3 52.7 all-gather.1
where the time goes:
time: 483 us; the launch traced here: 482 us
  blocking collectives  237 us (49%)
  waiting for transfers between devices  167 us (35%)
  starting transfers between devices  28.5 us (6%)
  local copies, waits for them, and re-layouts  17.8 us (4%)
  matrix products  13.9 us (3%)
  between operations  13.6 us (3%)
    all_to_all x1, blocking collectives, body(): lax.all_to_all(buffer, EP, split_axis=0, concat_axis=0, tiled=True)  200 us
    all_to_all x1, waiting for transfers between devices, moved_by_axis(): lax.all_to_all(blocks, axes[k], split_axis=k, concat_axis=k, tiled=True)  115 us
    all_gather x1, waiting for transfers between devices, body(): lax.all_gather(lax.all_to_all(buffer, EP, split_axis=0, concat_axis=0, ti...  52.9 us
    all_to_all x1, blocking collectives, copy_for_each(): lax.all_to_all(jnp.broadcast_to(array[None], (length, *array.shape)), axi...  31.1 us
    all_to_all x1, starting transfers between devices, moved_by_axis(): lax.all_to_all(blocks, axes[k], split_axis=k, concat_axis=k, tiled=True)  23.3 us
  transfers between devices with their start and end apart: 3, of which 2 were waited for; matrix products, arithmetic and copies ran while one was open for 1% of the time, Pallas kernels for 0%

commit v1 on v0

--- a/solution.py
+++ b/solution.py
@@ -6,6 +6,28 @@
 
 EP = ("ep_0", "ep_1")
 GRP_EP = ("grp", "ep_0", "ep_1")
+
+
+def joined_along(pieces, dim):
+    dims = list(pieces.shape[1:])
+    dims[dim] *= pieces.shape[0]
+    return jnp.moveaxis(pieces, 0, dim).reshape(dims)
+
+
+def collect_2(x, axis, dim):
+    size = lax.axis_size(axis)
+    pairs = [(i, (i + 1) % size) for i in range(size)]
+    back = [(b, a) for a, b in pairs]
+    lower, upper = ([], [])
+    for hop in range(size - 1):
+        if hop % 2 == 0:
+            lower.append(lax.ppermute(lower[-1] if lower else x, axis, pairs))
+        else:
+            upper.append(lax.ppermute(upper[-1] if upper else x, axis, back))
+    pieces = jnp.stack([*lower[::-1], x, *upper])
+    shift = lax.axis_index(axis) - len(lower)
+    pieces = pieces[(jnp.arange(size) - shift) % size]
+    return joined_along(pieces, dim)
 
 
 def copy_for_each(array, axis):
@@ -102,12 +124,7 @@
     normed = (values * inv_rms[:, None] * gain_piece[None, :]).astype(jnp.bfloat16)
     buffer = jnp.dot(dispatch, normed, preferred_element_type=jnp.float32).astype(jnp.bfloat16)
     buffer = buffer.reshape(ep_count, exp_local, capacity, piece_width)
-    piece = lax.all_gather(
-        lax.all_to_all(buffer, EP, split_axis=0, concat_axis=0, tiled=True),
-        "tp",
-        axis=3,
-        tiled=True,
-    )
+    piece = collect_2(lax.all_to_all(buffer, EP, split_axis=0, concat_axis=0, tiled=True), "tp", 3)
     gate_next = jnp.einsum("sxcd,xdf->sxcf", piece, w_gate, preferred_element_type=jnp.float32)
     up_next = jnp.einsum("sxcd,xdf->sxcf", piece, w_up, preferred_element_type=jnp.float32)
     results = finish_rows(gate_next, up_next, w_down)

time: 483 us -> 488 us (1.010)
  local copies, waits for them, and re-layouts: 17.8 us -> 46.9 us
  between operations: 13.6 us -> 0.26 us
  waiting for transfers between devices: 167 us -> 158 us
    all_gather x1 -> x0, waiting for transfers between devices: 52.9 us -> none  [body(): lax.all_gather(lax.all_to_all(buffer, EP, split_axis=0, concat_axis=0, ti...]
    ppermute x0 -> x3, waiting for transfers between devices: none -> 43.8 us  [the longest x2 43.8 us: collect_2(): lower.append(lax.ppermute(lower[-1] if lower else x, axis, pairs))]
    all_to_all x1, starting transfers between devices: 23.3 us -> 9.87 us  [moved_by_axis(): lax.all_to_all(blocks, axes[k], split_axis=k, concat_axis=k, tiled=True)]
    ppermute x0 -> x3, starting transfers between devices: none -> 8.95 us  [the longest x2 5.79 us: collect_2(): lower.append(lax.ppermute(lower[-1] if lower else x, axis, pairs))]
    another operation x1 -> x2, local copies, waits for them, and re-layouts: 2.9 us -> 11.7 us
    transpose x0 -> x1, local copies, waits for them, and re-layouts: none -> 8.64 us  [joined_along(): return jnp.moveaxis(pieces, 0, dim).reshape(dims)]
    gather x0 -> x1, local copies, waits for them, and re-layouts: none -> 6.39 us  [collect_2(): pieces = pieces[(jnp.arange(size) - shift) % size]]
    ppermute x0 -> x3, local copies, waits for them, and re-layouts: none -> 5.81 us  [the longest x2 3.88 us: collect_2(): lower.append(lax.ppermute(lower[-1] if lower else x, axis, pairs))]
  transfers between devices with their start and end apart: 3 -> 5, of which waited for: 2 -> 3; matrix products, arithmetic and copies ran while one was open for 1% -> 2% of each run, Pallas kernels for 0% -> 0%
where the time goes in v1:
time: 488 us; the launch traced here: 487 us
  blocking collectives  237 us (49%)
  waiting for transfers between devices  158 us (32%)
  local copies, waits for them, and re-layouts  46.9 us (10%)
  starting transfers between devices  23.9 us (5%)
  matrix products  13 us (3%)
  other arithmetic  8.19 us (2%)
    all_to_all x1, blocking collectives, body(): lax.all_to_all(buffer, EP, split_axis=0, concat_axis=0, tiled=True)  200 us
    all_to_all x1, waiting for transfers between devices, moved_by_axis(): lax.all_to_all(blocks, axes[k], split_axis=k, concat_axis=k, tiled=True)  115 us
    ppermute x2, waiting for transfers between devices, collect_2(): lower.append(lax.ppermute(lower[-1] if lower else x, axis, pairs))  43.8 us
    all_to_all x1, blocking collectives, copy_for_each(): lax.all_to_all(jnp.broadcast_to(array[None], (length, *array.shape)), axi...  27.7 us
    another operation x2, local copies, waits for them, and re-layouts  11.7 us
    all_to_all x1, starting transfers between devices, moved_by_axis(): lax.all_to_all(blocks, axes[k], split_axis=k, concat_axis=k, tiled=True)  9.87 us
  transfers between devices with their start and end apart: 5, of which 3 were waited for; matrix products, arithmetic and copies ran while one was open for 2% of the time, Pallas kernels for 0%

profile of v1, /device:TPU:33, one launch (start us, length us, event | category | flops | bytes accessed | tf_op | source)
XLA Modules:
  0.0 487.2 jit_solution(15552950663809139898)
XLA Ops:
  0.0 1.2 fusion.19
  1.2 0.6 broadcast_in_dim.6
  1.8 5.1 %all-to-all-start = ((f32[4,1,384]{2,1,0:T(1,128)}), f32[4,1,384]{2,1,0:T(1,128)S(1)}, u32[]{:S(2)}, u32[]{:S(2)}) async-start(f32[4,1,384]{2,1,0:T(1,128)} %broadcast_in_dim.6), calls=%async_computation | async-start | bytes 12288 | tf_op jit(solution)/shard_map/all_to_all | solution.py:35
  7.0 0.9 copy.44
  7.8 0.7 broadcast_multiply_fusion
  8.7 0.1 eq.87
  8.8 0.1 eq.83
  9.0 1.8 reduce-window.6
  10.8 0.3 slice_reduce_fusion.2
  11.1 0.1 fusion.27
  11.2 0.2 reduce_sum.40
  11.4 0.1 multiply_add_fusion
  11.5 0.3 slice_reduce_fusion.1
  11.8 0.8 dynamic_slice.3
  12.6 0.9 convolution_convert_fusion
  13.5 1.3 reshape.119
  14.8 199.7 %all_to_all.26 = bf16[64,1,18,512]{3,2,1,0:T(8,128)(2,1)S(1)} all-to-all(bf16[64,1,18,512]{3,2,1,0:T(8,128)(2,1)} %bitcast.98), channel_id=1, replica_groups=mesh['grp'=2,'ep_0'=32,'ep_1'=2,'tp'=4] {'ep_0','ep_1'}, dimensions={0} | all-to-all | bytes 2359296 | tf_op jit(solution)/shard_map/all_to_all | solution.py:127
  214.5 1.4 copy.48
  215.9 3.7 collective-permute-start
  219.6 3.2 collective-permute-start.2
  222.8 22.1 %collective-permute-done = bf16[64,1,18,512]{3,0,2,1:T(8,128)(2,1)} collective-permute-done((bf16[64,1,18,512]{3,0,2,1:T(8,128)(2,1)}, bf16[64,1,18,512]{3,0,2,1:T(8,128)(2,1)}, u32[]{:S(2)}, u32[]{:S(2)}) %collective-permute-start) | collective-permute-done | bytes 1179680 | tf_op jit(solution)/shard_map/ppermute | solution.py:24
  244.9 2.1 collective-permute-start.1
  247.0 1.9 copy.65
  249.0 1.9 copy.64
  250.9 21.7 %collective-permute-done.1 = bf16[64,1,18,512]{3,0,2,1:T(8,128)(2,1)} collective-permute-done((bf16[64,1,18,512]{3,0,2,1:T(8,128)(2,1)}, bf16[64,1,18,512]{3,0,2,1:T(8,128)(2,1)}, u32[]{:S(2)}, u32[]{:S(2)}) %collective-permute-start.1) | collective-permute-done | bytes 1179680 | tf_op jit(solution)/shard_map/ppermute | solution.py:24
  272.7 1.9 copy.66
  274.6 4.0 maximum_bitcast_fusion
  278.6 6.4 %gather_fusion = bf16[4,64,18,512]{3,2,1,0:T(8,128)(2,1)} fusion(bf16[4,64,18,512]{3,2,1,0:T(8,128)(2,1)} %maximum_bitcast_fusion, s32[1024]{0:T(1024)S(1)} %pad_clamp_fusion), kind=kCustom, calls=%fused_computation | custom fusion | bytes 9437200 | tf_op jit(solution)/shard_map/gather | solution.py:29
  285.0 8.6 %copy.53 = bf16[64,1,18,4,512]{4,3,0,2,1:T(4,128)(2,1)} copy(bf16[64,1,18,4,512]{4,2,0,3,1:T(8,128)(2,1)} %bitcast.92) | data formatting | bytes 9437184 | tf_op jit(solution)/shard_map/transpose | solution.py:14
  293.6 8.8 %reshape.120 = bf16[64,18,2048]{2,0,1:T(8,128)(2,1)} reshape(bf16[64,1,18,4,512]{4,3,0,2,1:T(4,128)(2,1)} %copy.53) | data formatting | bytes 9437184 | tf_op jit(solution)/shard_map/reshape.4
  302.5 3.9 convolution_bitcast_fusion.1
  306.4 0.1 copy-done.7
  306.5 1.5 fusion.11
  308.1 0.3 broadcast_in_dim.8
  308.4 27.7 %all_to_all.27 = bf16[4,64,1,18,256]{4,1,3,2,0:T(8,128)(2,1)S(1)} all-to-all(bf16[4,64,1,18,256]{4,1,3,2,0:T(8,128)(2,1)S(1)} %broadcast_in_dim.8), channel_id=1, replica_groups=mesh['grp'=2,'ep_0'=32,'ep_1'=2,'tp'=4] {'tp'}, dimensions={0} | all-to-all | bytes 4718592 | tf_op jit(solution)/shard_map/all_to_all | solution.py:35
  336.1 2.0 copy.54
  338.2 2.9 reshape.123
  341.1 3.1 fusion.4
  344.2 0.5 reshape_reshape.3
  344.7 0.2 copy.55
  344.9 9.2 %all_to_all.28 = bf16[32,2,1,1,18,512]{5,0,4,3,2,1:T(8,128)(2,1)S(1)} all-to-all(bf16[32,2,1,1,18,512]{5,0,4,3,2,1:T(8,128)(2,1)S(1)} %copy.55), channel_id=1, replica_groups=mesh['grp'=2,'ep_0'=32,'ep_1'=2,'tp'=4] {'ep_1'}, dimensions={1} | all-to-all | bytes 2359296 | tf_op jit(solution)/shard_map/all_to_all | solution.py:66
  354.1 2.3 copy.56
  356.3 9.9 %all-to-all-start.4 = ((bf16[32,2,1,1,18,512]{5,1,4,3,2,0:T(2,128)(2,1)}), bf16[32,2,1,1,18,512]{5,1,4,3,2,0:T(2,128)(2,1)}, u32[]{:S(2)}, u32[]{:S(2)}) async-start(bf16[32,2,1,1,18,512]{5,1,4,3,2,0:T(2,128)(2,1)} %copy.56), calls=%async_computation.4 | async-start | bytes 2359296 | tf_op jit(solution)/shard_map/all_to_all | solution.py:66
  366.3 114.5 %all-to-all-done.4 = bf16[32,2,1,1,18,512]{5,1,4,3,2,0:T(2,128)(2,1)} async-done(((bf16[32,2,1,1,18,512]{5,1,4,3,2,0:T(2,128)(2,1)}), bf16[32,2,1,1,18,512]{5,1,4,3,2,0:T(2,128)(2,1)}, u32[]{:S(2)}, u32[]{:S(2)}) %all-to-all-start.4) | async-done | bytes 1179680 | tf_op jit(solution)/shard_map/all_to_all | solution.py:66
  480.8 1.6 copy.57
  482.4 1.2 reshape_reshape_reshape.3
  483.6 2.1 fusion.9
  485.7 1.5 fusion.10
  (27 shorter events, 0.3 us)
Async XLA Ops:
  0.0 341.1 %copy-start = (bf16[1,1024,512]{2,1,0:T(8,128)(2,1)S(1)}, bf16[1,1024,512]{2,1,0:T(8,128)(2,1)}, u32[]{:S(2)}) copy-start(bf16[1,1024,512]{2,1,0:T(8,128)(2,1)} %param.17) | copy-start | bytes 3145732
  1.8 10.7 %all-to-all-start = ((f32[4,1,384]{2,1,0:T(1,128)}), f32[4,1,384]{2,1,0:T(1,128)S(1)}, u32[]{:S(2)}, u32[]{:S(2)}) async-start(f32[4,1,384]{2,1,0:T(1,128)} %broadcast_in_dim.6), calls=%async_computation | async-start | bytes 12288 | tf_op jit(solution)/shard_map/all_to_all | solution.py:35
  7.0 5.6 %copy-start.3 = (bf16[384,512]{1,0:T(8,128)(2,1)S(1)}, bf16[384,512]{1,0:T(8,128)(2,1)}, u32[]{:S(2)}) copy-start(bf16[384,512]{1,0:T(8,128)(2,1)} %param.9) | copy-start | bytes 1179652
  215.9 28.9 %collective-permute-start = (bf16[64,1,18,512]{3,0,2,1:T(8,128)(2,1)}, bf16[64,1,18,512]{3,0,2,1:T(8,128)(2,1)}, u32[]{:S(2)}, u32[]{:S(2)}) collective-permute-start(bf16[64,1,18,512]{3,0,2,1:T(8,128)(2,1)} %copy.48), channel_id=1, source_target_pairs={{0,1},{1,2},{2,3},{3,0},{4,5},{5,6},{6,7},{7,4},{8,9},{9,10},{10,1... | collective-permute-start | bytes 3538952 | tf_op jit(solution)/shard_map/ppermute | solution.py:24
  219.6 29.4 %collective-permute-start.2 = (bf16[64,1,18,512]{3,0,2,1:T(8,128)(2,1)}, bf16[64,1,18,512]{3,0,2,1:T(8,128)(2,1)}, u32[]{:S(2)}, u32[]{:S(2)}) collective-permute-start(bf16[64,1,18,512]{3,0,2,1:T(8,128)(2,1)} %copy.48), channel_id=1, source_target_pairs={{1,0},{2,1},{3,2},{0,3},{5,4},{6,5},{7,6},{4,7},{9,8},{10,9},{11,1... | collective-permute-start | bytes 3538952 | tf_op jit(solution)/shard_map/ppermute | solution.py:26
  244.9 27.8 %collective-permute-start.1 = (bf16[64,1,18,512]{3,0,2,1:T(8,128)(2,1)}, bf16[64,1,18,512]{3,0,2,1:T(8,128)(2,1)}, u32[]{:S(2)}, u32[]{:S(2)}) collective-permute-start(bf16[64,1,18,512]{3,0,2,1:T(8,128)(2,1)} %collective-permute-done), channel_id=1, source_target_pairs={{0,1},{1,2},{2,3},{3,0},{4,5},{5,6},{6,7},{7,4},{8,9},{9,10},{10,1... | collective-permute-start | bytes 3538952 | tf_op jit(solution)/shard_map/ppermute | solution.py:24
  293.6 8.8 %copy-start.6 = (bf16[1,2048,256]{2,1,0:T(8,128)(2,1)S(1)}, bf16[1,2048,256]{2,1,0:T(8,128)(2,1)}, u32[]{:S(2)}) copy-start(bf16[1,2048,256]{2,1,0:T(8,128)(2,1)} %param.15) | copy-start | bytes 3145732
  302.5 3.9 copy-start.1
  302.5 4.1 copy-start.7
  356.3 9.9 %copy-start.4 = (f32[384,2]{0,1:T(2,128)S(1)}, f32[384,2]{0,1:T(2,128)}, u32[]{:S(2)}) copy-start(f32[384,2]{0,1:T(2,128)} %param.13) | copy-start | bytes 9220
  356.3 9.9 %copy-start.5 = (f32[384]{0:T(512)S(1)}, f32[384]{0:T(512)}, u32[]{:S(2)}) copy-start(f32[384]{0:T(512)} %param.12) | copy-start | bytes 4612
  356.3 124.5 %all-to-all-start.4 = ((bf16[32,2,1,1,18,512]{5,1,4,3,2,0:T(2,128)(2,1)}), bf16[32,2,1,1,18,512]{5,1,4,3,2,0:T(2,128)(2,1)}, u32[]{:S(2)}, u32[]{:S(2)}) async-start(bf16[32,2,1,1,18,512]{5,1,4,3,2,0:T(2,128)(2,1)} %copy.56), calls=%async_computation.4 | async-start | bytes 2359296 | tf_op jit(solution)/shard_map/all_to_all | solution.py:66
  483.6 2.1 copy-start.2
